TPU v7x, 256 devices: a whole 4x4x8 slice. The times are simulated.
256 devices in a mesh: ep: 64 (over z, x, core), tp: 4 (over y).
Axes of the slice: x: 4, y: 4, z: 8, core: 2. Of those that a mesh axis runs over, the one named last changes fastest.
Arguments:
- mixer_input: bfloat16 [32768, 2048], P('ep'), may hold values from -5.5 to 5.5
- expert_input: bfloat16 [32768, 2048], P('ep'), may hold values from -6 to 6
- gain_mixer: float32 [2048], replicated, may hold values from 0.1 to 1.9
- gain_expert: float32 [2048], replicated, may hold values from 0.1 to 1.9
- query_weight: bfloat16 [2048, 1536], P(None, 'tp')
- key_weight: bfloat16 [2048, 256], P(None, 'tp')
- value_weight: bfloat16 [2048, 256], P(None, 'tp'), may hold values from -0.125 to 0.125
- sink_logits: float32 [24], P('tp'), may hold values from 2 to 6
- output_weight: bfloat16 [1536, 2048], P('tp'), may hold values from -0.75 to 0.75
- expert_choice: int32 [32768, 2], P('ep'), may hold values from 0 to 63, all different within a row; in each aligned block of 128 rows (0 to 127, 128 to 255, ...) at most 8 rows name the same one
- route_weights: float32 [32768, 2], P('ep'), may hold values from 0.2 to 1.2
- expert_gate: bfloat16 [64, 2048, 1024], P('ep', None, 'tp'), may hold values from -0.125 to 0.125
- expert_up: bfloat16 [64, 2048, 1024], P('ep', None, 'tp'), may hold values from -0.125 to 0.125
- expert_down: bfloat16 [64, 1024, 2048], P('ep', 'tp'), may hold values from -0.1875 to 0.1875
- shared_gate: bfloat16 [2048, 512], P(None, 'tp'), may hold values from -0.125 to 0.125
- shared_up: bfloat16 [2048, 512], P(None, 'tp'), may hold values from -0.125 to 0.125
- shared_down: bfloat16 [512, 2048], P('tp'), may hold values from -0.25 to 0.25
Outputs:
- mixer_output: bfloat16 [32768, 2048], P(('ep', 'tp'))
- expert_output: bfloat16 [32768, 2048], P(('ep', 'tp'))
Inputs may be any that keep to these rules, and one draw needn't show every extreme that they name: `expert_choice`: in each aligned block of 128 rows no expert is named by more than 8 rows, and in some block some expert is named by exactly 8 rows; the 2 entries of a row differ.
All inputs are finite; a program needn't handle non-finite values.
Results may differ from a plain program's by a relative error of at most 0.019.
Values may be sent and summed in bfloat16 or wider, within the bound.
A program may use at most 128 MiB of HBM per device.

v0:
```python
import math
import jax
import jax.numpy as jnp
from jax import lax
from jax.sharding import PartitionSpec as P

HEAD_DIM = 64
WINDOW = 128
SEQS = 1
norm_eps = 1e-06
rope_base = 500000.0


def from_behind(value, axis, steps):
    count = lax.axis_size(axis)
    first, last = (max(0, -steps), min(count, count - steps))
    return lax.ppermute(value, axis, [(source, source + steps) for source in range(first, last)])


def cut_along(shard, dim, count):
    lengths = shard.shape
    pieces = shard.reshape(*lengths[:dim], count, lengths[dim] // count, *lengths[dim + 1 :])
    return jnp.moveaxis(pieces, dim, 0)


def sent_and_summed(shard, axis, dim):
    pieces = cut_along(shard, dim, lax.axis_size(axis))
    arrived = lax.all_to_all(pieces, axis, split_axis=0, concat_axis=0, tiled=True)
    return arrived.astype(jnp.float32).sum(axis=0)


def rounded(value):
    return lax.optimization_barrier(value.astype(jnp.bfloat16)).astype(jnp.float32)


def rms_scale(matrix, scaling):
    widened = matrix.astype(jnp.float32)
    scaled = widened * lax.rsqrt(jnp.mean(widened * widened, axis=-1, keepdims=True) + norm_eps)
    return (scaled * scaling).astype(jnp.bfloat16)


def frequencies(head_size):
    half_steps = jnp.arange(head_size // 2, dtype=jnp.float32)
    return rope_base ** (-(2.0 * half_steps) / head_size)


def rotate(heads, angles):
    middle = heads.shape[-1] // 2
    widened = heads.astype(jnp.float32)
    cosine = jnp.cos(angles)[:, None, :]
    sine_val = jnp.sin(angles)[:, None, :]
    leading = widened[..., :middle]
    trailing = widened[..., middle:]
    turned = jnp.concatenate(
        [leading * cosine - trailing * sine_val, trailing * cosine + leading * sine_val], axis=-1
    )
    return turned.astype(jnp.bfloat16)


def attend(
    query_heads, key_heads, value_heads, prior_keys, prior_values, first_position, sink_logits
):
    window = prior_keys.shape[0]
    total_rows, kv_count, head_size = key_heads.shape
    group_size = query_heads.shape[1] // kv_count
    blocks = total_rows // window

    def banded(earlier, current):
        joined = jnp.concatenate([earlier, current], axis=0).reshape(
            blocks + 1, window, kv_count, head_size
        )
        return jnp.concatenate([joined[:-1], joined[1:]], axis=1)

    band_keys = banded(prior_keys, key_heads)
    band_values = banded(prior_values, value_heads)
    query_blocks = query_heads.reshape(blocks, window, kv_count, group_size, head_size)
    scores = jnp.einsum(
        "nqhgd,nkhd->nhgqk", query_blocks, band_keys, preferred_element_type=jnp.float32
    ) / math.sqrt(head_size)
    query_index = jnp.arange(window, dtype=jnp.int32)[:, None]
    key_index = jnp.arange(2 * window, dtype=jnp.int32)[None, :]
    distance = query_index + window - key_index
    block_start = first_position + jnp.arange(blocks, dtype=jnp.int32)[:, None, None] * window
    allowed = (distance >= 0) & (distance < window) & (block_start - window + key_index >= 0)
    scores = jnp.where(allowed[:, None, None, :, :], scores, -jnp.inf)
    sink_grid = sink_logits.reshape(kv_count, group_size)[None, :, :, None, None]
    row_peak = jnp.maximum(jnp.max(scores, axis=-1, keepdims=True), sink_grid)
    shifted_exp = jnp.exp(scores - row_peak)
    denominator = jnp.sum(shifted_exp, axis=-1, keepdims=True) + jnp.exp(sink_grid - row_peak)
    probs = (shifted_exp / denominator).astype(jnp.bfloat16)
    attended = jnp.einsum(
        "nhgqk,nkhd->nqhgd", probs, band_values, preferred_element_type=jnp.float32
    )
    return attended.astype(jnp.bfloat16).reshape(total_rows, kv_count * group_size * head_size)


def local(
    mixer_input,
    expert_input,
    gain_mixer,
    gain_expert,
    query_weight,
    key_weight,
    value_weight,
    sink_logits,
    output_weight,
    expert_choice,
    route_weights,
    expert_gate,
    expert_up,
    expert_down,
    shared_gate,
    shared_up,
    shared_down,
):
    tp_count = lax.axis_size("tp")
    ep_count = lax.axis_size("ep")
    tp_rank = lax.axis_index("tp")
    group_rows, model_width = mixer_input.shape
    normed = rms_scale(mixer_input, gain_mixer)
    queries = jnp.dot(normed, query_weight, preferred_element_type=jnp.float32).astype(jnp.bfloat16)
    key_rows = jnp.dot(normed, key_weight, preferred_element_type=jnp.float32).astype(jnp.bfloat16)
    value_rows = jnp.dot(normed, value_weight, preferred_element_type=jnp.float32).astype(
        jnp.bfloat16
    )
    first_position = lax.axis_index("ep") % (ep_count // SEQS) * group_rows
    positions = (first_position + jnp.arange(group_rows, dtype=jnp.int32)).astype(jnp.float32)
    angles = positions[:, None] * frequencies(HEAD_DIM)[None, :]
    rot_queries = rotate(queries.reshape(group_rows, -1, HEAD_DIM), angles)
    rot_keys = rotate(key_rows.reshape(group_rows, -1, HEAD_DIM), angles)
    key_width = key_rows.shape[1]
    tail_start = group_rows - WINDOW
    tail_pair = jnp.concatenate(
        [rot_keys.reshape(group_rows, key_width)[tail_start:], value_rows[tail_start:]], axis=1
    )
    earlier_pair = from_behind(tail_pair, "ep", 1)
    prior_keys = earlier_pair[:, :key_width].reshape(WINDOW, -1, HEAD_DIM)
    prior_values = earlier_pair[:, key_width:].reshape(WINDOW, -1, HEAD_DIM)
    attended = attend(
        rot_queries,
        rot_keys,
        value_rows.reshape(group_rows, -1, HEAD_DIM),
        prior_keys,
        prior_values,
        first_position,
        sink_logits,
    )
    picked = attended
    mixer_output = lax.psum_scatter(
        rounded(jnp.dot(picked, output_weight, preferred_element_type=jnp.float32)).astype(
            jnp.bfloat16
        ),
        "tp",
        scatter_dimension=0,
        tiled=True,
    )
    normed_rows = rms_scale(expert_input, gain_expert)
    group_tokens = normed_rows.shape[0]
    own_tokens = group_tokens // tp_count
    top_count = expert_choice.shape[1]
    local_experts = expert_gate.shape[0]
    experts_all = local_experts * ep_count
    capacity = 2 * own_tokens * top_count // experts_all
    assigned = own_tokens * top_count
    picked_experts = expert_choice.reshape(tp_count, assigned)
    onehot = (
        picked_experts[:, :, None] == jnp.arange(experts_all, dtype=jnp.int32)[None, None, :]
    ).astype(jnp.int32)
    slot_ranks = jnp.sum(jnp.cumsum(onehot, axis=1) * onehot, axis=-1) - 1
    padded_rows = jnp.concatenate([normed_rows, jnp.zeros((1, model_width), jnp.bfloat16)], axis=0)

    def own_slot_index():
        own_experts = lax.dynamic_index_in_dim(picked_experts, tp_rank, 0, keepdims=False)
        own_ranks = lax.dynamic_index_in_dim(slot_ranks, tp_rank, 0, keepdims=False)
        return own_experts * capacity + own_ranks

    own_owner = tp_rank * own_tokens + jnp.arange(assigned, dtype=jnp.int32) // top_count
    slot_table = (
        jnp.full((experts_all * capacity,), group_tokens, jnp.int32)
        .at[own_slot_index()]
        .set(own_owner)
    )
    outgoing = padded_rows[slot_table].reshape(experts_all, 1, capacity, model_width)
    arrived = lax.all_gather(
        lax.all_to_all(outgoing, "ep", split_axis=0, concat_axis=0, tiled=True),
        "tp",
        axis=1,
        tiled=True,
    )
    sources = arrived.shape[0] // local_experts
    shaped = arrived.reshape(
        sources, local_experts, arrived.shape[1], arrived.shape[2], arrived.shape[3]
    )
    gate_values = jnp.einsum(
        "iejcd,edf->iejcf", shaped, expert_gate, preferred_element_type=jnp.float32
    )
    up_values = jnp.einsum(
        "iejcd,edf->iejcf", shaped, expert_up, preferred_element_type=jnp.float32
    )
    hidden = (jax.nn.silu(gate_values) * up_values).astype(jnp.bfloat16)
    result = jnp.einsum("iejcf,efd->iejcd", hidden, expert_down, preferred_element_type=jnp.float32)
    partials = result.astype(jnp.bfloat16).reshape(arrived.shape)
    summed = sent_and_summed(partials.astype(jnp.float32).astype(jnp.bfloat16), "tp", 1)
    returned = (
        lax.all_to_all(summed.astype(jnp.bfloat16), "ep", split_axis=0, concat_axis=0, tiled=True)
        .astype(summed.dtype)
        .reshape(-1, model_width)
    )
    own_weights = lax.dynamic_slice_in_dim(route_weights, tp_rank * own_tokens, own_tokens, 0)
    gathered = returned[own_slot_index().reshape(own_tokens, top_count)]
    routed = jnp.sum(gathered * own_weights[:, :, None], axis=1)
    picked = normed_rows
    gate_values = jnp.dot(picked, shared_gate, preferred_element_type=jnp.float32)
    up_values = jnp.dot(picked, shared_up, preferred_element_type=jnp.float32)
    hidden = (jax.nn.silu(gate_values) * up_values).astype(jnp.bfloat16)
    shared_part = lax.psum_scatter(
        rounded(jnp.dot(hidden, shared_down, preferred_element_type=jnp.float32)).astype(
            jnp.bfloat16
        ),
        "tp",
        scatter_dimension=0,
        tiled=True,
    ).astype(jnp.float32)
    expert_output = (routed + shared_part).astype(jnp.bfloat16)
    return (mixer_output, expert_output)


def solution(mesh):
    placed = (
        P("ep", None),
        P("ep", None),
        P(),
        P(),
        P(None, "tp"),
        P(None, "tp"),
        P(None, "tp"),
        P("tp"),
        P("tp", None),
        P("ep", None),
        P("ep", None),
        P("ep", None, "tp"),
        P("ep", None, "tp"),
        P("ep", "tp", None),
        P(None, "tp"),
        P(None, "tp"),
        P("tp", None),
    )
    return jax.shard_map(
        local,
        mesh=mesh,
        in_specs=placed,
        out_specs=(P(("ep", "tp"), None), P(("ep", "tp"), None)),
        check_vma=False,
    )
```

profile of v0, /device:TPU:2, one launch (start us, length us, event | category | flops | bytes accessed | tf_op | source)
XLA Modules:
  0.0 415.3 jit_solution(7231487003897511812)
XLA Ops:
  7.2 0.9 copy.50
  8.2 0.2 reshape.445
  8.4 0.2 eq.28
  8.5 2.1 fusion.3
  10.7 2.4 reduce-window.6
  13.1 0.1 slice.78
  13.4 0.2 fusion.38
  13.5 0.5 broadcast.319
  14.0 0.7 fusion.83
  14.7 1.4 scatter_custom_fusion
  16.1 2.1 fusion.5
  18.3 1.4 copy-done.1
  19.7 1.5 concatenate.64
  21.2 7.1 %gather_fusion = bf16[512,2048]{1,0:T(8,128)(2,1)} fusion(bf16[513,2048]{1,0:T(8,128)(2,1)} %concatenate.64, s32[1024]{0:T(1024)S(1)} %pad_clamp_fusion.1), kind=kCustom, calls=%fused_computation | custom fusion | bytes 4196352 | tf_op jit(solution)/shard_map/gather | solution.py:183
  28.3 63.5 %all_to_all.15 = bf16[64,1,8,2048]{3,2,1,0:T(8,128)(2,1)} all-to-all(bf16[64,1,8,2048]{3,2,1,0:T(8,128)(2,1)} %bitcast.203), channel_id=1, replica_groups=mesh['ep'=64,'tp'=4] {'ep'}, dimensions={0} | all-to-all | bytes 4194304 | tf_op jit(solution)/shard_map/all_to_all | solution.py:185
  91.8 82.2 %all-gather.2.cloned.1.call-done = bf16[64,4,8,2048]{3,2,1,0:T(8,128)(2,1)} async-done(((bf16[64,1,8,2048]{3,2,1,0:T(8,128)(2,1)}), bf16[64,4,8,2048]{3,2,1,0:T(8,128)(2,1)}) %all-gather.2.cloned.1.call-update) | async-done | bytes 8388624 | tf_op jit(solution)/shard_map/all_gather | solution.py:184
  174.0 7.1 %fusion.27 = f32[64,4,8,256]{3,2,1,0:T(8,128)} fusion(bf16[64,4,8,2048]{3,2,1,0:T(8,128)(2,1)} %all-gather.2.cloned.1.call-done, bf16[1,2048,256]{2,1,0:T(8,128)(2,1)S(1)} %copy-done.10), kind=kOutput, calls=%fused_computation.45 | convolution fusion | flops 2147483648 | bytes 11534336 | tf_op jit(solution)/shard_map/iejcd,edf->iejcf/dot_general | solution.py:194
  181.1 13.7 %convert_bitcast_fusion = bf16[4,64,1,8,2048]{4,3,0,1,2:T(8,128)(2,1)} fusion(bf16[1,256,2048]{2,1,0:T(8,128)(2,1)} %param.30, bf16[64,4,8,2048]{3,2,1,0:T(8,128)(2,1)} %all-gather.2.cloned.1.call-done, f32[64,4,8,256]{3,2,1,0:T(8,128)} %fusion.27, bf16[1,2048,256]{2,1,0:T(8,128)(2,1)} %param.29), kind=kOutput, calls=%fused_computation.3 | convolution fusion | flops 4302307328 | bytes 20971520 | tf_op jit(solution)/shard_map/iejcf,efd->iejcd/dot_general | solution.py:201
  194.8 8.3 %copy.55 = bf16[4,64,1,8,2048]{4,3,1,2,0:T(8,128)(2,1)} copy(bf16[4,64,1,8,2048]{4,3,0,1,2:T(8,128)(2,1)} %convert_bitcast_fusion) | data formatting | bytes 16777216 | tf_op jit(solution)/shard_map/transpose | solution.py:23
  203.1 5.7 %all-to-all-start.1 = ((bf16[4,64,1,8,2048]{4,3,1,2,0:T(8,128)(2,1)}), bf16[4,64,1,8,2048]{4,3,1,2,0:T(8,128)(2,1)}, u32[]{:S(2)}, u32[]{:S(2)}) async-start(bf16[4,64,1,8,2048]{4,3,1,2,0:T(8,128)(2,1)} %copy.55), calls=%async_computation.2 | async-start | bytes 16777216 | tf_op jit(solution)/shard_map/all_to_all | solution.py:28
  208.8 2.1 fusion
  211.0 2.6 convolution_convert_fusion.3
  213.6 0.8 fusion.24
  214.5 0.3 fusion.62
  214.8 2.1 collective-permute-start
  217.0 0.7 fusion.85
  217.7 5.3 %convolution_convert_fusion = bf16[512,2048]{1,0:T(8,128)(2,1)} fusion(bf16[128,2048]{1,0:T(8,128)(2,1)S(1)} %copy-done.6, bf16[512,2048]{1,0:T(8,128)(2,1)} %copy-done.1, bf16[2048,128]{1,0:T(8,128)(2,1)S(1)} %copy-done.7, f32[512,128]{1,0:T(8,128)S(1)} %fusion.85), kind=kOutput, calls=%fused_computation.17 | convolution fusion | flops 538312704 | bytes 5505024 | tf_op jit(solution)/shard_map/dot_general | solution.py:217
  223.0 3.2 convolution_convert_fusion.2
  226.4 0.3 multiply_cosine_fusion
  226.7 0.2 broadcast_and_fusion
  227.3 2.3 fusion.7
  229.7 89.8 %all-to-all-done.1 = bf16[4,64,1,8,2048]{4,3,1,2,0:T(8,128)(2,1)} async-done(((bf16[4,64,1,8,2048]{4,3,1,2,0:T(8,128)(2,1)}), bf16[4,64,1,8,2048]{4,3,1,2,0:T(8,128)(2,1)}, u32[]{:S(2)}, u32[]{:S(2)}) %all-to-all-start.1) | async-done | bytes 8388640 | tf_op jit(solution)/shard_map/all_to_all | solution.py:28
  319.5 7.3 %reduce_sum.63 = bf16[64,8,2048]{2,1,0:T(8,128)(2,1)} reduce(bf16[4,64,1,8,2048]{4,3,1,2,0:T(8,128)(2,1)} %all-to-all-done.1, bf16[]{:T(256)} %constant.96.clone.1), dimensions={0,2}, to_apply=%region_9.10 | reduce | flops 3145728 | bytes 10485762 | tf_op jit(solution)/shard_map/reduce_sum | solution.py:29
  326.8 10.7 %all-to-all-start.2 = ((bf16[64,1,8,2048]{3,2,1,0:T(8,128)(2,1)}), bf16[64,1,8,2048]{3,2,1,0:T(8,128)(2,1)}, u32[]{:S(2)}, u32[]{:S(2)}) async-start(bf16[64,1,8,2048]{3,2,1,0:T(8,128)(2,1)} %bitcast.204), calls=%async_computation.3 | async-start | bytes 4194304 | tf_op jit(solution)/shard_map/all_to_all | solution.py:205
  337.5 0.3 reduce-scatter.3.cloned.1.call-start
  337.8 2.7 fusion.6
  340.7 1.0 fusion.19
  341.6 0.3 copy.49
  341.9 2.6 convolution_convert_fusion.1
  344.6 0.7 constant_dynamic-slice_fusion
  345.4 0.1 add.207
  345.5 0.1 reshape.469
  345.7 43.0 %all-to-all-done.2 = bf16[64,1,8,2048]{3,2,1,0:T(8,128)(2,1)} async-done(((bf16[64,1,8,2048]{3,2,1,0:T(8,128)(2,1)}), bf16[64,1,8,2048]{3,2,1,0:T(8,128)(2,1)}, u32[]{:S(2)}, u32[]{:S(2)}) %all-to-all-start.2) | async-done | bytes 2097184 | tf_op jit(solution)/shard_map/all_to_all | solution.py:205
  388.7 4.0 bitcast_convert_fusion
  392.7 5.8 %gather_fusion.1 = f32[256,2048]{1,0:T(8,128)} fusion(f32[512,2048]{1,0:T(8,128)} %bitcast_convert_fusion, s32[1024]{0:T(1024)S(1)} %pad_clamp_fusion), kind=kCustom, calls=%fused_computation.1 | custom fusion | bytes 4195328 | tf_op jit(solution)/shard_map/gather | solution.py:210
  398.5 3.5 reshape.468
  402.0 4.7 %multiply_reduce_fusion = f32[128,2048]{1,0:T(8,128)S(1)} fusion(f32[128,2,2048]{2,1,0:T(2,128)} %reshape.468, f32[128,2]{1,0:T(8,128)S(1)} %copy.56), kind=kLoop, calls=%fused_computation.29 | loop fusion | flops 786432 | bytes 3146752 | tf_op jit(solution)/shard_map/reduce_sum | solution.py:211
  406.8 1.9 add_convert_fusion
  (70 shorter events, 1.3 us)
Async XLA Ops:
  7.2 334.8 %copy-start = (bf16[384,2048]{1,0:T(8,128)(2,1)S(1)}, bf16[384,2048]{1,0:T(8,128)(2,1)}, u32[]{:S(2)}) copy-start(bf16[384,2048]{1,0:T(8,128)(2,1)} %param.25) | copy-start | bytes 4718596
  7.2 166.8 %all-gather.2.cloned.1.call-start = ((), (), s32[]{:S(2)}) async-start(), calls=%async_computation.6 | async-start | bytes 10485760 | tf_op jit(solution)/shard_map/all_gather | solution.py:184
  8.3 7.8 %copy-start.8 = (f32[2048]{0:T(1024)S(1)}, f32[2048]{0:T(1024)}, u32[]{:S(2)}) copy-start(f32[2048]{0:T(1024)} %param.20) | copy-start | bytes 24580
  18.3 1.4 copy-start.1
  28.3 145.7 %copy-start.10 = (bf16[1,2048,256]{2,1,0:T(8,128)(2,1)S(1)}, bf16[1,2048,256]{2,1,0:T(8,128)(2,1)}, u32[]{:S(2)}) copy-start(bf16[1,2048,256]{2,1,0:T(8,128)(2,1)} %param.28) | copy-start | bytes 3145732
  203.1 116.4 %all-to-all-start.1 = ((bf16[4,64,1,8,2048]{4,3,1,2,0:T(8,128)(2,1)}), bf16[4,64,1,8,2048]{4,3,1,2,0:T(8,128)(2,1)}, u32[]{:S(2)}, u32[]{:S(2)}) async-start(bf16[4,64,1,8,2048]{4,3,1,2,0:T(8,128)(2,1)} %copy.55), calls=%async_computation.2 | async-start | bytes 16777216 | tf_op jit(solution)/shard_map/all_to_all | solution.py:28
  208.7 2.2 copy-start.11
  208.7 2.2 copy-start.13
  208.8 198.0 %reduce-scatter.5.cloned.1.call-start = ((), (), s32[]{:S(2)}) async-start(), calls=%async_computation.7 | async-start | bytes 2621440 | tf_op jit(solution)/shard_map/reduce_scatter | solution.py:216
  210.9 2.7 copy-start.4
  210.9 2.7 copy-start.12
  213.6 3.4 copy-start.2
  213.6 3.4 copy-start.5
  214.4 3.3 copy-start.6
  214.4 3.3 copy-start.7
  214.8 12.4 %collective-permute-start = (bf16[128,128]{0,1:T(8,128)(2,1)S(1)}, bf16[128,128]{0,1:T(8,128)(2,1)S(1)}, u32[]{:S(2)}, u32[]{:S(2)}) collective-permute-start(bf16[128,128]{0,1:T(8,128)(2,1)S(1)} %pad_maximum_fusion.3), channel_id=1, source_target_pairs={{0,4},{4,8},{8,12},{12,16},{16,20},{20,24},{24,28},{28,32},{32,36}... | collective-permute-start | bytes 98312 | tf_op jit(solution)/shard_map/ppermute | solution.py:17
  227.3 2.3 copy-start.9
  326.8 61.9 %all-to-all-start.2 = ((bf16[64,1,8,2048]{3,2,1,0:T(8,128)(2,1)}), bf16[64,1,8,2048]{3,2,1,0:T(8,128)(2,1)}, u32[]{:S(2)}, u32[]{:S(2)}) async-start(bf16[64,1,8,2048]{3,2,1,0:T(8,128)(2,1)} %bitcast.204), calls=%async_computation.3 | async-start | bytes 4194304 | tf_op jit(solution)/shard_map/all_to_all | solution.py:205
  337.5 71.2 %reduce-scatter.3.cloned.1.call-start = ((), (), s32[]{:S(2)}) async-start(), calls=%async_computation.5 | async-start | bytes 2621440 | tf_op jit(solution)/shard_map/reduce_scatter | solution.py:149
  337.8 2.8 copy-start.3
Sparse Core Ops, SparseCore 0:
  91.9 81.9 all-gather.1
  223.1 51.7 reduce-scatter.4
  344.7 31.4 reduce-scatter.2
where the time goes:
time: 416 us; the launch traced here: 415 us
  waiting for transfers between devices  215 us (52%)
  blocking collectives  63.5 us (15%)
  matrix products  39.2 us (9%)
  local copies, waits for them, and re-layouts  32.7 us (8%)
  other arithmetic  31.7 us (8%)
  starting transfers between devices  18.9 us (5%)
  between operations  14.3 us (3%)
    all_to_all x1, waiting for transfers between devices, sent_and_summed(): lax.all_to_all(pieces, axis, split_axis=0, concat_axis=0, tiled=True)  89.8 us
    all_gather x1, waiting for transfers between devices, local(): lax.all_gather(lax.all_to_all(outgoing, 'ep', split_axis=0, concat_axis=0...  82.2 us
    all_to_all x1, blocking collectives, local(): lax.all_to_all(outgoing, 'ep', split_axis=0, concat_axis=0, tiled=True)  63.5 us
    all_to_all x1, waiting for transfers between devices, local(): lax.all_to_all(summed.astype(jnp.bfloat16), 'ep', split_axis=0, concat_ax...  43 us
    dot_general x1, matrix products, local(): jnp.einsum('iejcf,efd->iejcd', hidden, expert_down, preferred_element_typ...  13.7 us
    all_to_all x1, starting transfers between devices, local(): lax.all_to_all(summed.astype(jnp.bfloat16), 'ep', split_axis=0, concat_ax...  10.7 us
    gather x2, local copies, waits for them, and re-layouts, local(): gathered = returned[own_slot_index().reshape(own_tokens, top_count)]  9.32 us
  transfers between devices with their start and end apart: 6, of which 3 were waited for; matrix products, arithmetic and copies ran while one was open for 13% of the time, Pallas kernels for 0%

commit v1 on v0

--- a/solution.py
+++ b/solution.py
@@ -113,6 +113,14 @@
     shared_up,
     shared_down,
 ):
+
+    def shards_save(vals):
+        which_axis = "tp"
+        wide_n = jax.lax.axis_size(which_axis)
+        carry = jnp.tile(vals, [wide_n if dev == 1 else 1 for dev in range(vals.ndim)])
+        h_now = jax.lax.all_to_all(carry, which_axis, split_axis=1, concat_axis=1, tiled=True)
+        return h_now
+
     tp_count = lax.axis_size("tp")
     ep_count = lax.axis_size("ep")
     tp_rank = lax.axis_index("tp")
@@ -181,12 +189,7 @@
         .set(own_owner)
     )
     outgoing = padded_rows[slot_table].reshape(experts_all, 1, capacity, model_width)
-    arrived = lax.all_gather(
-        lax.all_to_all(outgoing, "ep", split_axis=0, concat_axis=0, tiled=True),
-        "tp",
-        axis=1,
-        tiled=True,
-    )
+    arrived = shards_save(lax.all_to_all(outgoing, "ep", split_axis=0, concat_axis=0, tiled=True))
     sources = arrived.shape[0] // local_experts
     shaped = arrived.reshape(
         sources, local_experts, arrived.shape[1], arrived.shape[2], arrived.shape[3]

time: 416 us -> 427 us (1.026)
  blocking collectives: 63.5 us -> 160 us
  waiting for transfers between devices: 215 us -> 130 us
    all_to_all x0 -> x1, blocking collectives: none -> 96.6 us  [shards_save(): jax.lax.all_to_all(carry, which_axis, split_axis=1, concat_axis=1, tiled=...]
    all_gather x1 -> x0, waiting for transfers between devices: 82.2 us -> none  [local(): lax.all_gather(lax.all_to_all(outgoing, 'ep', split_axis=0, concat_axis=0...]
  transfers between devices with their start and end apart: 6 -> 5, of which waited for: 3 -> 2; matrix products, arithmetic and copies ran while one was open for 13% -> 13% of each run, Pallas kernels for 0% -> 0%
where the time goes in v1:
time: 427 us
  blocking collectives  160 us (37%)
  waiting for transfers between devices  130 us (30%)
  local copies, waits for them, and re-layouts  36.9 us (9%)
  matrix products  35.3 us (8%)
  other arithmetic  31.8 us (7%)
  starting transfers between devices  17.7 us (4%)
  between operations  14.6 us (3%)
    all_to_all x1, blocking collectives, shards_save(): jax.lax.all_to_all(carry, which_axis, split_axis=1, concat_axis=1, tiled=...  96.6 us
    all_to_all x1, waiting for transfers between devices, sent_and_summed(): lax.all_to_all(pieces, axis, split_axis=0, concat_axis=0, tiled=True)  87.3 us
    all_to_all x1, blocking collectives, local(): lax.all_to_all(outgoing, 'ep', split_axis=0, concat_axis=0, tiled=True)  63.3 us
    all_to_all x1, waiting for transfers between devices, local(): lax.all_to_all(summed.astype(jnp.bfloat16), 'ep', split_axis=0, concat_ax...  43 us
    dot_general x1, matrix products, local(): jnp.einsum('iejcf,efd->iejcd', hidden, expert_down, preferred_element_typ...  13.4 us
    all_to_all x1, starting transfers between devices, local(): lax.all_to_all(summed.astype(jnp.bfloat16), 'ep', split_axis=0, concat_ax...  9.46 us
    gather x2, local copies, waits for them, and re-layouts, local(): gathered = returned[own_slot_index().reshape(own_tokens, top_count)]  9.32 us
  transfers between devices with their start and end apart: 5, of which 2 were waited for; matrix products, arithmetic and copies ran while one was open for 13% of the time, Pallas kernels for 0%

profile of v1, /device:TPU:2, one launch (start us, length us, event | category | flops | bytes accessed | tf_op | source)
XLA Modules:
  0.0 426.6 jit_solution(12229963479963203300)
XLA Ops:
  7.2 0.9 copy.50
  8.1 0.2 reshape.448
  8.3 0.2 eq.28
  8.5 2.1 fusion.7
  10.6 2.4 reduce-window.6
  13.3 0.2 fusion.47
  13.5 0.5 broadcast.321
  14.0 0.7 fusion.92
  14.7 1.4 scatter_custom_fusion
  16.1 2.1 fusion.9
  18.3 1.3 copy-done.1
  19.6 1.5 concatenate.64
  21.1 7.1 %gather_fusion = bf16[512,2048]{1,0:T(8,128)(2,1)} fusion(bf16[513,2048]{1,0:T(8,128)(2,1)} %concatenate.64, s32[1024]{0:T(1024)S(1)} %pad_clamp_fusion.1), kind=kCustom, calls=%fused_computation | custom fusion | bytes 4196352 | tf_op jit(solution)/shard_map/gather | solution.py:191
  28.2 63.3 %all_to_all.20 = bf16[64,1,8,2048]{3,2,1,0:T(8,128)(2,1)S(1)} all-to-all(bf16[64,1,8,2048]{3,2,1,0:T(8,128)(2,1)} %bitcast.203), channel_id=1, replica_groups=mesh['ep'=64,'tp'=4] {'ep'}, dimensions={0} | all-to-all | bytes 4194304 | tf_op jit(solution)/shard_map/all_to_all | solution.py:192
  91.5 1.1 tile.10
  92.6 96.6 %all_to_all.21 = bf16[64,4,8,2048]{3,2,0,1:T(8,128)(2,1)S(1)} all-to-all(bf16[64,4,8,2048]{3,2,0,1:T(8,128)(2,1)S(1)} %tile.10), channel_id=1, replica_groups=mesh['ep'=64,'tp'=4] {'tp'}, dimensions={1} | all-to-all | bytes 16777216 | tf_op jit(solution)/shard_map/all_to_all | solution.py:121
  189.2 3.2 copy-done.3
  192.4 3.6 fusion.2
  196.0 13.4 %convert_bitcast_fusion = bf16[4,64,1,8,2048]{4,3,0,1,2:T(8,128)(2,1)} fusion(bf16[64,4,8,2048]{3,2,0,1:T(8,128)(2,1)} %copy-done.3, f32[64,4,8,256]{3,2,1,0:T(8,128)} %fusion.2, bf16[1,256,2048]{2,1,0:T(8,128)(2,1)S(1)} %copy-done.12, bf16[1,2048,256]{2,1,0:T(8,128)(2,1)} %param.29), kind=kOutput, calls=%fused_computation.3 | convolution fusion | flops 4302307328 | bytes 20971520 | tf_op jit(solution)/shard_map/iejcf,efd->iejcd/dot_general | solution.py:204
  209.5 8.3 %copy.58 = bf16[4,64,1,8,2048]{4,3,1,2,0:T(8,128)(2,1)} copy(bf16[4,64,1,8,2048]{4,3,0,1,2:T(8,128)(2,1)} %convert_bitcast_fusion) | data formatting | bytes 16777216 | tf_op jit(solution)/shard_map/transpose | solution.py:23
  217.7 5.8 %all-to-all-start.2 = ((bf16[4,64,1,8,2048]{4,3,1,2,0:T(8,128)(2,1)}), bf16[4,64,1,8,2048]{4,3,1,2,0:T(8,128)(2,1)}, u32[]{:S(2)}, u32[]{:S(2)}) async-start(bf16[4,64,1,8,2048]{4,3,1,2,0:T(8,128)(2,1)} %copy.58), calls=%async_computation.3 | async-start | bytes 16777216 | tf_op jit(solution)/shard_map/all_to_all | solution.py:28
  223.6 2.2 fusion.4
  225.9 2.4 convolution_convert_fusion.3
  228.4 0.8 fusion.34
  229.2 0.3 fusion.71
  229.6 2.1 collective-permute-start
  231.8 0.7 fusion.94
  232.5 5.3 %convolution_convert_fusion = bf16[512,2048]{1,0:T(8,128)(2,1)} fusion(bf16[128,2048]{1,0:T(8,128)(2,1)S(1)} %copy-done.7, bf16[512,2048]{1,0:T(8,128)(2,1)} %copy-done.1, bf16[2048,128]{1,0:T(8,128)(2,1)S(1)} %copy-done.8, f32[512,128]{1,0:T(8,128)S(1)} %fusion.94), kind=kOutput, calls=%fused_computation.21 | convolution fusion | flops 538312704 | bytes 5505024 | tf_op jit(solution)/shard_map/dot_general | solution.py:220
  237.8 3.2 convolution_convert_fusion.2
  241.2 0.3 multiply_cosine_fusion
  241.5 0.2 broadcast_and_fusion
  242.1 2.3 fusion.11
  244.5 87.3 %all-to-all-done.2 = bf16[4,64,1,8,2048]{4,3,1,2,0:T(8,128)(2,1)} async-done(((bf16[4,64,1,8,2048]{4,3,1,2,0:T(8,128)(2,1)}), bf16[4,64,1,8,2048]{4,3,1,2,0:T(8,128)(2,1)}, u32[]{:S(2)}, u32[]{:S(2)}) %all-to-all-start.2) | async-done | bytes 8388640 | tf_op jit(solution)/shard_map/all_to_all | solution.py:28
  331.8 7.3 %reduce_sum.63 = bf16[64,8,2048]{2,1,0:T(8,128)(2,1)} reduce(bf16[4,64,1,8,2048]{4,3,1,2,0:T(8,128)(2,1)} %all-to-all-done.2, bf16[]{:T(256)} %constant.96.clone.1), dimensions={0,2}, to_apply=%region_9.10 | reduce | flops 3145728 | bytes 10485762 | tf_op jit(solution)/shard_map/reduce_sum | solution.py:29
  339.1 9.5 %all-to-all-start.3 = ((bf16[64,1,8,2048]{3,2,1,0:T(8,128)(2,1)}), bf16[64,1,8,2048]{3,2,1,0:T(8,128)(2,1)}, u32[]{:S(2)}, u32[]{:S(2)}) async-start(bf16[64,1,8,2048]{3,2,1,0:T(8,128)(2,1)} %bitcast.205), calls=%async_computation.4 | async-start | bytes 4194304 | tf_op jit(solution)/shard_map/all_to_all | solution.py:208
  348.5 0.3 reduce-scatter.3.cloned.1.call-start
  348.9 2.7 fusion.10
  351.7 1.0 fusion.27
  352.6 0.3 copy.49
  353.0 2.6 convolution_convert_fusion.1
  355.6 0.7 constant_dynamic-slice_fusion
  356.6 0.1 reshape.472
  356.7 43.0 %all-to-all-done.3 = bf16[64,1,8,2048]{3,2,1,0:T(8,128)(2,1)} async-done(((bf16[64,1,8,2048]{3,2,1,0:T(8,128)(2,1)}), bf16[64,1,8,2048]{3,2,1,0:T(8,128)(2,1)}, u32[]{:S(2)}, u32[]{:S(2)}) %all-to-all-start.3) | async-done | bytes 2097184 | tf_op jit(solution)/shard_map/all_to_all | solution.py:208
  399.7 4.0 bitcast_convert_fusion
  403.7 5.8 %gather_fusion.1 = f32[256,2048]{1,0:T(8,128)} fusion(f32[512,2048]{1,0:T(8,128)} %bitcast_convert_fusion, s32[1024]{0:T(1024)S(1)} %pad_clamp_fusion), kind=kCustom, calls=%fused_computation.1 | custom fusion | bytes 4195328 | tf_op jit(solution)/shard_map/gather | solution.py:213
  409.5 3.5 reshape.471
  413.1 4.7 %multiply_reduce_fusion = f32[128,2048]{1,0:T(8,128)S(1)} fusion(f32[128,2,2048]{2,1,0:T(2,128)} %reshape.471, f32[128,2]{1,0:T(8,128)S(1)} %copy.59), kind=kLoop, calls=%fused_computation.33 | loop fusion | flops 786432 | bytes 3146752 | tf_op jit(solution)/shard_map/reduce_sum | solution.py:214
  417.8 1.9 add_convert_fusion
  (73 shorter events, 1.5 us)
Async XLA Ops:
  7.2 345.8 %copy-start = (bf16[384,2048]{1,0:T(8,128)(2,1)S(1)}, bf16[384,2048]{1,0:T(8,128)(2,1)}, u32[]{:S(2)}) copy-start(bf16[384,2048]{1,0:T(8,128)(2,1)} %param.25) | copy-start | bytes 4718596
  7.2 8.9 %copy-start.9 = (f32[2048]{0:T(1024)S(1)}, f32[2048]{0:T(1024)}, u32[]{:S(2)}) copy-start(f32[2048]{0:T(1024)} %param.20) | copy-start | bytes 24580
  18.3 1.4 copy-start.1
  92.6 99.8 %copy-start.11 = (bf16[1,2048,256]{2,1,0:T(8,128)(2,1)S(1)}, bf16[1,2048,256]{2,1,0:T(8,128)(2,1)}, u32[]{:S(2)}) copy-start(bf16[1,2048,256]{2,1,0:T(8,128)(2,1)} %param.28) | copy-start | bytes 3145732
  189.2 3.2 copy-start.3
  192.4 3.6 copy-start.12
  217.7 8.1 %copy-start.13 = (bf16[2048,64]{0,1:T(8,128)(2,1)S(1)}, bf16[2048,64]{0,1:T(8,128)(2,1)}, u32[]{:S(2)}) copy-start(bf16[2048,64]{0,1:T(8,128)(2,1)} %param.23) | copy-start | bytes 786436
  217.7 8.1 %copy-start.15 = (f32[2048]{0:T(1024)S(1)}, f32[2048]{0:T(1024)}, u32[]{:S(2)}) copy-start(f32[2048]{0:T(1024)} %param.19) | copy-start | bytes 24580
  217.7 114.1 %all-to-all-start.2 = ((bf16[4,64,1,8,2048]{4,3,1,2,0:T(8,128)(2,1)}), bf16[4,64,1,8,2048]{4,3,1,2,0:T(8,128)(2,1)}, u32[]{:S(2)}, u32[]{:S(2)}) async-start(bf16[4,64,1,8,2048]{4,3,1,2,0:T(8,128)(2,1)} %copy.58), calls=%async_computation.3 | async-start | bytes 16777216 | tf_op jit(solution)/shard_map/all_to_all | solution.py:28
  223.5 4.8 %copy-start.14 = (bf16[2048,64]{0,1:T(8,128)(2,1)S(1)}, bf16[2048,64]{0,1:T(8,128)(2,1)}, u32[]{:S(2)}) copy-start(bf16[2048,64]{0,1:T(8,128)(2,1)} %param.22) | copy-start | bytes 786436
  223.5 194.3 %reduce-scatter.5.cloned.1.call-start = ((), (), s32[]{:S(2)}) async-start(), calls=%async_computation.7 | async-start | bytes 2621440 | tf_op jit(solution)/shard_map/reduce_scatter | solution.py:219
  223.6 4.8 %copy-start.5 = (bf16[512,2048]{1,0:T(8,128)(2,1)S(1)}, bf16[512,2048]{1,0:T(8,128)(2,1)}, u32[]{:S(2)}) copy-start(bf16[512,2048]{1,0:T(8,128)(2,1)} %param.17) | copy-start | bytes 6291460
  228.3 3.5 copy-start.2
  228.3 3.5 copy-start.6
  228.4 4.1 copy-start.7
  228.4 4.1 copy-start.8
  229.6 12.4 %collective-permute-start = (bf16[128,128]{0,1:T(8,128)(2,1)S(1)}, bf16[128,128]{0,1:T(8,128)(2,1)S(1)}, u32[]{:S(2)}, u32[]{:S(2)}) collective-permute-start(bf16[128,128]{0,1:T(8,128)(2,1)S(1)} %pad_maximum_fusion.3), channel_id=1, source_target_pairs={{0,4},{4,8},{8,12},{12,16},{16,20},{20,24},{24,28},{28,32},{32,36}... | collective-permute-start | bytes 98312 | tf_op jit(solution)/shard_map/ppermute | solution.py:17
  241.9 2.5 copy-start.10
  339.1 60.6 %all-to-all-start.3 = ((bf16[64,1,8,2048]{3,2,1,0:T(8,128)(2,1)}), bf16[64,1,8,2048]{3,2,1,0:T(8,128)(2,1)}, u32[]{:S(2)}, u32[]{:S(2)}) async-start(bf16[64,1,8,2048]{3,2,1,0:T(8,128)(2,1)} %bitcast.205), calls=%async_computation.4 | async-start | bytes 4194304 | tf_op jit(solution)/shard_map/all_to_all | solution.py:208
  348.5 71.2 %reduce-scatter.3.cloned.1.call-start = ((), (), s32[]{:S(2)}) async-start(), calls=%async_computation.6 | async-start | bytes 2621440 | tf_op jit(solution)/shard_map/reduce_scatter | solution.py:157
  348.9 2.8 copy-start.4
Sparse Core Ops, SparseCore 0:
  237.9 50.0 reduce-scatter.4
  355.7 31.4 reduce-scatter.2
